TPU v7x, 128 devices: a whole 4x4x4 slice. The times are simulated.
128 devices in a mesh: sp: 16 (over z, y), fs: 4 (over x), tp: 2 (over core).
Axes of the slice: x: 4, y: 4, z: 4, core: 2. Of those that a mesh axis runs over, the one named last changes fastest.
Arguments:
- hidden_in: bfloat16 [32768, 2048], P(('fs', 'sp'), 'tp'), parts along dimension 0, may hold values from -6 to 48
- in_gain: float32 [2048], replicated, may hold values from 0.1 to 1.9
- w_query: bfloat16 [2048, 1024], P(None, 'tp'), may hold values from -0.29972302 to 0.29972302
- w_key: bfloat16 [2048, 1024], P(None, 'tp'), may hold values from -0.29972302 to 0.29972302
- w_value: bfloat16 [2048, 1024], P(None, 'tp'), may hold values from -0.125 to 0.125
- w_gate: bfloat16 [2048, 1024], P(None, 'tp'), may hold values from -0.125 to 0.125
- w_inner: bfloat16 [2048, 1024], P(None, 'tp'), may hold values from -0.125 to 0.125
- w_bvec: bfloat16 [2048, 512], P(None, 'tp'), may hold values from -0.125 to 0.125
- w_cvec: bfloat16 [2048, 512], P(None, 'tp'), may hold values from -0.125 to 0.125
- w_step: bfloat16 [2048, 16], P(None, 'tp'), may hold values from -0.125 to 0.125
- conv_inner: bfloat16 [4, 1024], P(None, 'tp'), may hold values from -3 to 3
- conv_bvec: bfloat16 [4, 512], P(None, 'tp'), may hold values from -3 to 3
- conv_cvec: bfloat16 [4, 512], P(None, 'tp'), may hold values from -3 to 3
- a_log: float32 [16], P('tp'), may hold values from -16 to 0
- decay_add: float32 [32768, 16], P(('fs', 'sp'), 'tp'), parts along dimension 0, may hold values from -1 to 0
- lambdas: float32 [4], P('tp'), may hold values from 0.3 to 0.8
- head_gain: float32 [256], replicated, may hold values from 0.1 to 1.9
- ssm_gain: float32 [1024], P('tp'), may hold values from 0.1 to 1.9
- out_attn: bfloat16 [1024, 2048], P('tp'), may hold values from -0.125 to 0.125
- out_ssm: bfloat16 [1024, 2048], P('tp'), may hold values from -0.125 to 0.125
Outputs:
- layer_out: bfloat16 [32768, 2048], P(('fs', 'sp', 'tp')), parts along dimension 0
There are 4 independent parts, one for each index of `fs`. A program takes and returns all parts, laid end to end along the dimension named above; an argument that names none is the same for every part. Nothing has to cross between parts.
All inputs are finite; a program needn't handle non-finite values.
Results may differ from a plain program's by a relative error of at most 0.012.
The roundings to bfloat16 on the way count: a program that leaves them out, or rounds other values in their place, can miss the bound.
Values may be sent and summed in bfloat16 or wider, within the bound.
A program may use at most 128 MiB of HBM per device.

v0:
```python
import jax
import jax.numpy as jnp
from jax import lax
from jax.sharding import Mesh
from jax.sharding import PartitionSpec as P

D = 2048
QK_DIM = 128
SSM_P = 64
STATE = 128
BLOCK = 128
KEY_BLOCK = 128
SP = ("sp_0", "sp_1")
FS_SP = ("fs", "sp_0", "sp_1")
FS_SP_TP = ("fs", "sp_0", "sp_1", "tp")
EPS = 1e-06
NEG = -1e30


def gathered_total(x, axis):
    return lax.all_gather(x, axis).sum(0)


def laid_out(parts, dim):
    lengths = list(parts.shape[1:])
    lengths[dim] *= parts.shape[0]
    return jnp.moveaxis(parts, 0, dim).reshape(lengths)


def copy_for_each(x, axis):
    length = lax.axis_size(axis)
    return lax.all_to_all(jnp.broadcast_to(x[None], (length, *x.shape)), axis, 0, 0, tiled=True)


def collect(x, axis, dim):
    return laid_out(copy_for_each(x, axis), dim)


def from_behind(x, axis, by):
    length = lax.axis_size(axis)
    pairs = [(i, i + by) for i in range(length) if 0 <= i + by < length]
    return lax.ppermute(x, axis, pairs)


def nothing_yet(x, identity):
    return jax.tree.map(
        lambda a, e: jnp.broadcast_to(jnp.asarray(e, a.dtype), a.shape), x, identity
    )


def prefix_by_axis(x, axes, combine, identity):
    before = start = nothing_yet(x, identity)
    running = x
    for axis in reversed(axes):
        length, index = (lax.axis_size(axis), lax.axis_index(axis))
        pieces = jax.tree.map(
            lambda part, kind: lax.all_gather(part.astype(kind), axis),
            running,
            (jnp.bfloat16, jnp.bfloat16),
        )
        inside, running = (start, start)
        for k in range(length):
            passed = k < index
            running = combine(
                running, jax.tree.map(lambda part, own: part[k].astype(own.dtype), pieces, x)
            )
            inside = jax.tree.map(lambda new, old: jnp.where(passed, new, old), running, inside)
        before = combine(inside, before)
    return before


def side_by_side(arrays, axis, dim, along):
    both = jnp.concatenate(arrays, axis=along)
    filled, at, gathered = (lax.all_gather(both, axis, axis=dim, tiled=True), 0, [])
    for a in arrays:
        gathered.append(lax.slice_in_dim(filled, at, at + a.shape[along], axis=along))
        at += a.shape[along]
    return tuple(gathered)


def per_device(
    hidden_in,
    in_gain,
    w_query,
    w_key,
    w_value,
    w_gate,
    w_inner,
    w_bvec,
    w_cvec,
    w_step,
    conv_inner,
    conv_bvec,
    conv_cvec,
    a_log,
    decay_add,
    lambdas,
    head_gain,
    ssm_gain,
    out_attn,
    out_ssm,
):
    rows_dev, half_width = hidden_in.shape
    in_float = hidden_in.astype(jnp.float32)
    squares = gathered_total(jnp.sum(in_float * in_float, axis=1), "tp")
    gain_half = lax.dynamic_slice_in_dim(in_gain, lax.axis_index("tp") * half_width, half_width, 0)
    normed = (in_float * lax.rsqrt(squares[:, None] / D + EPS) * gain_half[None, :]).astype(
        jnp.bfloat16
    )
    whole = collect(normed, "tp", 1)
    weight_list = (w_query, w_key, w_value, w_gate, w_inner, w_bvec, w_cvec, w_step)
    query, keys, values, gate_z, inner, b_pre, c_pre, step_pre = [
        jnp.dot(whole, weight, preferred_element_type=jnp.float32).astype(jnp.bfloat16)
        for weight in weight_list
    ]
    heads_att = lambdas.shape[0]
    first_row = lax.axis_index(SP) * rows_dev
    own_pos = first_row + jnp.arange(rows_dev, dtype=jnp.int32)
    scale = QK_DIM ** (-0.5)

    def head_major(rows_mat):
        return rows_mat.reshape(rows_mat.shape[0], heads_att * 2, QK_DIM).transpose(1, 0, 2)

    keys_major = head_major(keys)
    values_major = values.reshape(rows_dev, heads_att, 2 * QK_DIM).transpose(1, 0, 2)
    groups = [(head_major(query), own_pos)]
    start_states = tuple(
        (
            (
                jnp.full((heads_att, 2, group_pos.shape[0]), NEG, jnp.float32),
                jnp.zeros((heads_att, 2, group_pos.shape[0]), jnp.float32),
                jnp.zeros((heads_att, 2, group_pos.shape[0], 2 * QK_DIM), jnp.float32),
            )
            for group_query, group_pos in groups
        )
    )
    key_piece = lax.all_gather(keys_major, SP, axis=1, tiled=True)
    value_piece = lax.all_gather(values_major, SP, axis=1, tiled=True)

    def one_block(block_index, states):
        key_start = block_index * KEY_BLOCK
        key_rows = lax.dynamic_slice_in_dim(key_piece, block_index * KEY_BLOCK, KEY_BLOCK, 1)
        value_rows = lax.dynamic_slice_in_dim(value_piece, block_index * KEY_BLOCK, KEY_BLOCK, 1)
        key_pos = key_start + jnp.arange(KEY_BLOCK, dtype=jnp.int32)
        results = []
        for (group_query, group_pos), state in zip(groups, states):
            query_count = group_pos.shape[0]

            def update(current):
                peak, totals, accum = current
                scores = (
                    jnp.einsum(
                        "mqd,mkd->mqk", group_query, key_rows, preferred_element_type=jnp.float32
                    ).reshape(heads_att, 2, query_count, KEY_BLOCK)
                    * scale
                )
                visible = (key_pos[None, :] <= group_pos[:, None])[None, None]
                new_peak = jnp.maximum(peak, jnp.max(jnp.where(visible, scores, NEG), axis=-1))
                weights = jnp.where(visible, jnp.exp(scores - new_peak[..., None]), 0.0)
                shrink = jnp.exp(peak - new_peak)
                totals = totals * shrink + jnp.sum(weights, axis=-1)
                accum = accum * shrink[..., None] + jnp.einsum(
                    "hmqk,hke->hmqe",
                    weights.astype(jnp.bfloat16),
                    value_rows,
                    preferred_element_type=jnp.float32,
                )
                return (new_peak, totals, accum)

            results.append(
                lax.cond(key_start <= group_pos[-1], update, lambda unchanged: unchanged, state)
            )
        return tuple(results)

    finals = lax.fori_loop(0, key_piece.shape[1] // KEY_BLOCK, one_block, start_states)
    outputs = []
    for peak, totals, accum in finals:
        first_map = accum[:, 0] / totals[:, 0, :, None]
        second_map = accum[:, 1] / totals[:, 1, :, None]
        differ = first_map - lambdas[:, None, None] * second_map
        head_norm = (
            differ * lax.rsqrt(jnp.mean(differ * differ, axis=-1, keepdims=True) + EPS) * head_gain
        )
        outputs.append(
            head_norm.astype(jnp.bfloat16)
            .transpose(1, 0, 2)
            .reshape(accum.shape[2], heads_att * 2 * QK_DIM)
        )
    attn_out = outputs[0]
    heads_ssm = a_log.shape[0]
    groups_local = b_pre.shape[1] // STATE
    per_group = heads_ssm // groups_local
    stacked = jnp.concatenate([inner, b_pre, c_pre], axis=1)
    taps = conv_inner.shape[0]
    earlier = from_behind(stacked[rows_dev - (taps - 1) :], SP, 1)
    padded = jnp.concatenate([earlier, stacked], axis=0).astype(jnp.float32)
    conv_weight = jnp.concatenate([conv_inner, conv_bvec, conv_cvec], axis=1).astype(jnp.float32)
    summed = padded[0:rows_dev] * conv_weight[0]
    for offset in range(1, taps):
        summed = summed + padded[offset : offset + rows_dev] * conv_weight[offset]
    activated = jax.nn.silu(summed).astype(jnp.bfloat16)
    width_inner = inner.shape[1]
    width_vec = b_pre.shape[1]
    block_count = rows_dev // BLOCK
    inputs_x = activated[:, :width_inner].reshape(block_count, BLOCK, heads_ssm, SSM_P)
    inputs_b = activated[:, width_inner : width_inner + width_vec].reshape(
        block_count, BLOCK, groups_local, STATE
    )
    inputs_c = activated[:, width_inner + width_vec :].reshape(
        block_count, BLOCK, groups_local, STATE
    )
    step_size = jax.nn.softplus(step_pre.astype(jnp.float32))
    log_decay = -jnp.exp(a_log)[None, :] * step_size + decay_add
    size_major = step_size.reshape(block_count, BLOCK, heads_ssm).transpose(0, 2, 1)
    running = jnp.cumsum(
        log_decay.reshape(block_count, BLOCK, heads_ssm).transpose(0, 2, 1), axis=2
    )
    causal = jnp.tril(jnp.ones((BLOCK, BLOCK), dtype=bool))
    decay = jnp.exp(
        jnp.where(causal[None, None], running[:, :, :, None] - running[:, :, None, :], NEG)
    )
    intersection = jnp.einsum(
        "ntgk,nsgk->ngts", inputs_c, inputs_b, preferred_element_type=jnp.float32
    )
    matrix = (
        jnp.repeat(intersection, per_group, axis=1) * decay * size_major[:, :, None, :]
    ).astype(jnp.bfloat16)
    inside = jnp.einsum("nhts,nshp->nthp", matrix, inputs_x, preferred_element_type=jnp.float32)
    to_end = (jnp.exp(running[:, :, -1:] - running) * size_major).transpose(0, 2, 1)
    weighted = (inputs_x.astype(jnp.float32) * to_end[..., None]).astype(jnp.bfloat16)
    heads_b = jnp.repeat(inputs_b, per_group, axis=2)
    fresh = jnp.einsum("nshp,nshk->nhpk", weighted, heads_b, preferred_element_type=jnp.float32)
    block_totals = running[:, :, -1]

    def chain(state, items):
        fresh_block, total_block = items
        return (state * jnp.exp(total_block)[:, None, None] + fresh_block, state)

    local_end, local_enter = lax.scan(
        chain, jnp.zeros((heads_ssm, SSM_P, STATE), jnp.float32), (fresh, block_totals)
    )
    device_total = jnp.sum(block_totals, axis=0)

    def link(before, after):
        return (before[0] * jnp.exp(after[1])[:, None, None] + after[0], before[1] + after[1])

    incoming, skipped = prefix_by_axis(
        (local_end, device_total),
        SP,
        link,
        (jnp.zeros_like(local_end), jnp.zeros_like(device_total)),
    )
    preceding = jnp.concatenate(
        [jnp.zeros((1, heads_ssm), jnp.float32), jnp.cumsum(block_totals, axis=0)[:-1]], axis=0
    )
    entering = local_enter + incoming[None] * jnp.exp(preceding)[:, :, None, None]
    heads_c = jnp.repeat(inputs_c, per_group, axis=2).astype(jnp.float32)
    carried = (
        jnp.einsum("nthk,nhpk->nthp", heads_c, entering, precision=lax.Precision.HIGHEST)
        * jnp.exp(running).transpose(0, 2, 1)[..., None]
    )
    ssm_y = (inside + carried).reshape(rows_dev, heads_ssm * SSM_P)
    gated = (ssm_y * jax.nn.silu(gate_z.astype(jnp.float32))).reshape(rows_dev, groups_local, -1)
    grouped = gated * lax.rsqrt(jnp.mean(gated * gated, axis=-1, keepdims=True) + EPS)
    ssm_out = (grouped.reshape(rows_dev, heads_ssm * SSM_P) * ssm_gain).astype(jnp.bfloat16)
    attn_rows, ssm_rows = (
        lax.all_to_all(attn_out, "tp", split_axis=0, concat_axis=1, tiled=True),
        lax.all_to_all(ssm_out, "tp", split_axis=0, concat_axis=1, tiled=True),
    )
    full_attn, full_ssm = side_by_side((out_attn, out_ssm), "tp", 0, 1)
    joined = jnp.dot(attn_rows, full_attn, preferred_element_type=jnp.float32) + jnp.dot(
        ssm_rows, full_ssm, preferred_element_type=jnp.float32
    )
    return joined.astype(jnp.bfloat16)


def solution(mesh):
    split = Mesh(
        mesh.devices.reshape(4, 4, mesh.shape["fs"], mesh.shape["tp"]), ("sp_0", "sp_1", "fs", "tp")
    )
    in_specs = (
        P(FS_SP, "tp"),
        P(),
        P(None, "tp"),
        P(None, "tp"),
        P(None, "tp"),
        P(None, "tp"),
        P(None, "tp"),
        P(None, "tp"),
        P(None, "tp"),
        P(None, "tp"),
        P(None, "tp"),
        P(None, "tp"),
        P(None, "tp"),
        P("tp"),
        P(FS_SP, "tp"),
        P("tp"),
        P(),
        P("tp"),
        P("tp", None),
        P("tp", None),
    )
    out_specs = P(FS_SP_TP, None)
    return jax.shard_map(
        per_device, mesh=split, in_specs=in_specs, out_specs=out_specs, check_vma=False
    )
```

profile of v0, /device:TPU:127, one launch (start us, length us, event | category | flops | bytes accessed | tf_op | source)
XLA Modules:
  0.0 632.4 jit_solution(1211561122861284005)
XLA Ops:
  18.1 5.5 all_to_all.43
  43.7 7.7 %all-reduce.1 = bf16[32]{0:T(256)(128)(2,1)S(1)} all-reduce(bf16[32]{0:T(256)(128)(2,1)S(1)} %dynamic-update-slice), channel_id=3, replica_groups=mesh['sp_0'=4,'sp_1'=4,'fs'=4,'tp'=2] {'sp_1'}, use_global_device_ids=true, to_apply=%add.1 | all-reduce | flops 32 | bytes 128
  77.0 7.2 %while.31 = (s32[]{:T(128)}, f32[8,64,128]{2,1,0:T(8,128)S(1)}, f32[4,8,64,128]{3,2,1,0:T(8,128)}, f32[4,8]{1,0:T(4,128)S(1)}, f32[4,8,64,128]{3,2,1,0:T(8,128)}, /*index=5*/s32[]{:T(128)}, s32[]{:T(128)}) while((s32[]{:T(128)}, f32[8,64,128]{2,1,0:T(8,128)S(1)}, f32[4,8,64,128]{3,2,1,0:T(8,128)}, f32[4,8]{1,0:T(4,128)S(1)}, ...), condition=%wide.region_11.12_spmd.clone, body=%wide.region_10.11_spmd.clone.sunk | while | flops 262147 | bytes 1311424 | solution.py:239
  85.5 14.2 %all-gather.2 = bf16[32,64,128]{2,1,0:T(8,128)(2,1)S(1)} all-gather(bf16[8,64,128]{2,1,0:T(8,128)(2,1)S(1)} %convert_element_type.242), channel_id=4, replica_groups=mesh['sp_0'=4,'sp_1'=4,'fs'=4,'tp'=2] {'sp_1'}, dimensions={0}, use_global_device_ids=true | all-gather | bytes 655360 | tf_op jit(solution)/shard_map/all_gather | solution.py:57
  100.6 12.0 %all_gather.42 = bf16[4,8,64,128]{3,2,1,0:T(8,128)(2,1)S(1)} all-gather(bf16[1,8,64,128]{3,2,1,0:T(8,128)(2,1)S(1)} %fusion.62), channel_id=1, replica_groups=mesh['sp_0'=4,'sp_1'=4,'fs'=4,'tp'=2] {'sp_0'}, dimensions={0}, use_global_device_ids=true | all-gather | bytes 655360 | tf_op jit(solution)/shard_map/all_gather | solution.py:57
  134.0 10.5 %all_to_all.44 = bf16[2,256,512]{1,2,0:T(8,128)(2,1)S(1)} all-to-all(bf16[2,256,512]{1,2,0:T(8,128)(2,1)S(1)} %copy.107), channel_id=1, replica_groups=mesh['sp_0'=4,'sp_1'=4,'fs'=4,'tp'=2] {'tp'}, dimensions={0} | all-to-all | bytes 1048576 | tf_op jit(solution)/shard_map/all_to_all | solution.py:268
  149.3 34.8 %all-gather.9.cloned.1.call-done = bf16[4,8192,128]{2,1,0:T(8,128)(2,1)} async-done(((bf16[4,512,128]{2,1,0:T(8,128)(2,1)}), bf16[4,8192,128]{2,1,0:T(8,128)(2,1)}) %all-gather.9.cloned.1.call-update) | async-done | bytes 8388624 | tf_op jit(solution)/shard_map/all_gather | solution.py:137
  185.7 426.3 %while.30 = (s32[]{:T(128)}, f32[2,2,512]{2,1,0:T(2,128)S(1)}, f32[2,2,512]{2,1,0:T(2,128)S(1)}, f32[2,2,512,256]{3,2,1,0:T(8,128)}, s32[512]{0:T(512)S(1)}, /*i...) while((s32[]{:T(128)}, f32[2,2,512]{2,1,0:T(2,128)S(1)}, ...), condition=%wide.region_7.8_spmd, body=%wide.region_2.7_spmd.sunk | while | flops 204804224 | bytes 10801461 | solution.py:175
  193.8 5.3 conditional.2
  200.4 5.3 conditional.2
  207.1 5.3 conditional.2
  213.8 5.3 conditional.2
  220.4 5.3 conditional.2
  227.1 5.3 conditional.2
  233.7 5.3 conditional.2
  240.4 5.3 conditional.2
  247.1 5.3 conditional.2
  253.7 5.3 conditional.2
  260.4 5.3 conditional.2
  267.0 5.3 conditional.2
  273.7 5.3 conditional.2
  280.4 5.3 conditional.2
  287.0 5.3 conditional.2
  293.7 5.3 conditional.2
  300.3 5.3 conditional.2
  307.0 5.3 conditional.2
  313.7 5.3 conditional.2
  320.3 5.3 conditional.2
  327.0 5.3 conditional.2
  333.7 5.3 conditional.2
  340.3 5.3 conditional.2
  347.0 5.3 conditional.2
  353.6 5.3 conditional.2
  360.3 5.3 conditional.2
  367.0 5.3 conditional.2
  373.6 5.3 conditional.2
  380.3 5.3 conditional.2
  386.9 5.3 conditional.2
  393.6 5.3 conditional.2
  413.6 5.3 conditional.2
  433.6 5.3 conditional.2
  466.9 5.3 conditional.2
  486.9 5.3 conditional.2
  506.8 5.3 conditional.2
  520.2 5.3 conditional.2
  540.1 5.3 conditional.2
  560.1 5.3 conditional.2
  593.4 5.3 conditional.2
  (1150 shorter events, 611.0 us)
Async XLA Ops:
  6.5 118.4 %copy-start = (bf16[2048,512]{1,0:T(8,128)(2,1)S(1)}, bf16[2048,512]{1,0:T(8,128)(2,1)}, u32[]{:S(2)}) copy-start(bf16[2048,512]{1,0:T(8,128)(2,1)} %param.31) | copy-start | bytes 6291460
  6.5 138.0 %all-gather.13.cloned.1.call-start = ((), (), s32[]{:S(2)}) async-start(), calls=%async_computation.5 | async-start | bytes 12582912 | tf_op jit(solution)/shard_map/all_gather | solution.py:74
  11.4 0.7 copy-start.21
  11.4 1.2 copy-start.4
  11.4 137.9 %all-gather.11.cloned.1.call-start = ((), (), s32[]{:S(2)}) async-start(), calls=%async_computation.4 | async-start | bytes 8912896 | tf_op jit(solution)/shard_map/all_gather | solution.py:138
  18.0 6.9 %copy-start.25 = (bf16[2048,512]{1,0:T(8,128)(2,1)S(1)}, bf16[2048,512]{1,0:T(8,128)(2,1)}, u32[]{:S(2)}) copy-start(bf16[2048,512]{1,0:T(8,128)(2,1)} %param.30) | copy-start | bytes 6291460
  23.6 1.3 copy-start.2
  27.3 156.8 %all-gather.9.cloned.1.call-start = ((), (), s32[]{:S(2)}) async-start(), calls=%async_computation.3 | async-start | bytes 8912896 | tf_op jit(solution)/shard_map/all_gather | solution.py:137
  32.3 2.8 copy-start.3
  32.4 2.8 copy-start.27
  35.2 3.0 copy-start.8
  35.2 1.7 copy-start.26
  36.9 1.3 copy-start.9
  36.9 3.5 copy-start.28
  36.9 3.5 copy-start.14
  38.2 2.6 copy-start.15
  38.2 3.8 copy-start.29
  38.2 19.7 %copy-start.18 = (bf16[4,512]{1,0:T(4,128)(2,1)S(1)}, bf16[4,512]{1,0:T(4,128)(2,1)}, u32[]{:S(2)}) copy-start(bf16[4,512]{1,0:T(4,128)(2,1)} %param.36) | copy-start | bytes 12292
  38.2 19.7 %copy-start.19 = (bf16[4,256]{1,0:T(4,128)(2,1)S(1)}, bf16[4,256]{1,0:T(4,128)(2,1)}, u32[]{:S(2)}) copy-start(bf16[4,256]{1,0:T(4,128)(2,1)} %param.38) | copy-start | bytes 6148
  38.2 19.7 %copy-start.20 = (bf16[4,256]{1,0:T(4,128)(2,1)S(1)}, bf16[4,256]{1,0:T(4,128)(2,1)}, u32[]{:S(2)}) copy-start(bf16[4,256]{1,0:T(4,128)(2,1)} %param.37) | copy-start | bytes 6148
  39.1 27.0 %collective-permute-start = (bf16[3,1024]{0,1:T(8,128)(2,1)}, bf16[3,1024]{0,1:T(8,128)(2,1)}, u32[]{:S(2)}, u32[]{:S(2)}) collective-permute-start(bf16[3,1024]{0,1:T(8,128)(2,1)} %pad_maximum_fusion.1), channel_id=1, source_target_pairs={{0,8},{8,16},{16,24},{24,32},{32,40},{40,48},{48,56},{56,64},{64,7... | collective-permute-start | bytes 18440 | tf_op jit(solution)/shard_map/ppermute | solution.py:42
  40.8 23.4 %copy-start.10 = (f32[512,8]{0,1:T(8,128)}, f32[512,8]{0,1:T(8,128)S(1)}, u32[]{:S(2)}) copy-start(f32[512,8]{0,1:T(8,128)S(1)} %compare_select_fusion) | copy-start | bytes 49156
  113.7 1.0 copy-start.5
  113.7 1.0 copy-start.11
  113.7 1.0 copy-start.16
  114.7 1.2 copy-start.7
  114.7 1.2 copy-start.13
  114.7 1.2 copy-start.17
  132.3 1.3 copy-start.6
  132.3 1.2 copy-start.22
  149.3 36.4 %copy-start.12 = (s32[512]{0:T(512)S(1)}, s32[512]{0:T(512)}, u32[]{:S(2)}) copy-start(s32[512]{0:T(512)} %iota_add_fusion) | copy-start | bytes 6148
  185.7 426.4 %copy-start.24 = (f32[2]{0:T(128)S(1)}, f32[2]{0:T(128)}, u32[]{:S(2)}) copy-start(f32[2]{0:T(128)} %param.41) | copy-start | bytes 28
  612.1 2.1 copy-start.23
  620.6 5.3 copy-start.1
Sparse Core Ops, SparseCore 0:
  11.5 24.0 all-gather.12
  37.8 73.6 all-gather.10
  113.6 70.4 all-gather.8
where the time goes:
time: 637 us; the launch traced here: 632 us
  matrix products  313 us (49%)
  local copies, waits for them, and re-layouts  106 us (17%)
  blocking collectives  62.5 us (10%)
  other arithmetic  50.5 us (8%)
  loops' own time  49.6 us (8%)
  waiting for transfers between devices  34.9 us (5%)
  between operations  14.3 us (2%)
    dot_general x64, matrix products, update(): jnp.einsum('hmqk,hke->hmqe', weights.astype(jnp.bfloat16), value_rows, pr...  196 us
    dot_general x64, matrix products, update(): jnp.einsum('mqd,mkd->mqk', group_query, key_rows, preferred_element_type=...  80.3 us
    another operation x1, loops' own time, per_device(): lax.fori_loop(0, key_piece.shape[1] // KEY_BLOCK, one_block, start_states)  44.8 us
    slice x64, local copies, waits for them, and re-layouts, one_block(): group_pos[-1]  42.2 us
    all_gather x1, waiting for transfers between devices, per_device(): key_piece = lax.all_gather(keys_major, SP, axis=1, tiled=True)  34.8 us
    all_gather x3, blocking collectives, prefix_by_axis(): lax.all_gather(part.astype(kind), axis)  31.5 us
    mul x64, local copies, waits for them, and re-layouts, update(): jnp.einsum('mqd,mkd->mqk', group_query, key_rows, preferred_element_type=...  20.7 us
    dot_general x8, matrix products, per_device(): jnp.dot(whole, weight, preferred_element_type=jnp.float32)  19.7 us
  transfers between devices with their start and end apart: 4, of which 1 were waited for; matrix products, arithmetic and copies ran while one was open for 12% of the time, Pallas kernels for 0%

commit v1 on v0

--- a/solution.py
+++ b/solution.py
@@ -15,6 +15,13 @@
 FS_SP_TP = ("fs", "sp_0", "sp_1", "tp")
 EPS = 1e-06
 NEG = -1e30
+
+
+def all_by_exchange(value, name, dim):
+    size = lax.axis_size(name)
+    shards = jnp.stack([value for _ in range(size)])
+    shards = lax.all_to_all(shards, name, split_axis=0, concat_axis=0)
+    return jnp.concatenate(shards, axis=dim)
 
 
 def gathered_total(x, axis):
@@ -134,7 +141,7 @@
             for group_query, group_pos in groups
         )
     )
-    key_piece = lax.all_gather(keys_major, SP, axis=1, tiled=True)
+    key_piece = all_by_exchange(keys_major, SP, 1)
     value_piece = lax.all_gather(values_major, SP, axis=1, tiled=True)
 
     def one_block(block_index, states):

time: 637 us -> 747 us (1.17)
  blocking collectives: 62.5 us -> 184 us
  waiting for transfers between devices: 34.9 us -> 0.04 us
  starting transfers between devices: 1.36 us -> 22.2 us
  local copies, waits for them, and re-layouts: 106 us -> 115 us
    unnamed x1, blocking collectives: 7.68 us -> 144 us
    all_gather x1 -> x0, waiting for transfers between devices: 34.8 us -> none  [per_device(): key_piece = lax.all_gather(keys_major, SP, axis=1, tiled=True)]
    all_to_all x0 -> x2, starting transfers between devices: none -> 20.9 us  [the longest x1 14.5 us: per_device(): lax.all_to_all(ssm_out, 'tp', split_axis=0, concat_axis=1, tiled=True)]
    all_to_all x1 -> x0, blocking collectives: 10.5 us -> none  [per_device(): lax.all_to_all(ssm_out, 'tp', split_axis=0, concat_axis=1, tiled=True)]
    all_to_all x0 -> x1, local copies, waits for them, and re-layouts: none -> 7.74 us  [all_by_exchange(): shards = lax.all_to_all(shards, name, split_axis=0, concat_axis=0)]
  transfers between devices with their start and end apart: 4 -> 5, of which waited for: 1 -> 0; matrix products, arithmetic and copies ran while one was open for 12% -> 12% of each run, Pallas kernels for 0% -> 0%
where the time goes in v1:
time: 747 us; the launch traced here: 743 us
  matrix products  311 us (42%)
  blocking collectives  184 us (25%)
  local copies, waits for them, and re-layouts  115 us (15%)
  other arithmetic  50.6 us (7%)
  loops' own time  45 us (6%)
  starting transfers between devices  22.2 us (3%)
  between operations  14.6 us (2%)
    dot_general x64, matrix products, update(): jnp.einsum('hmqk,hke->hmqe', weights.astype(jnp.bfloat16), value_rows, pr...  195 us
    unnamed x1, blocking collectives  144 us
    dot_general x64, matrix products, update(): jnp.einsum('mqd,mkd->mqk', group_query, key_rows, preferred_element_type=...  80.2 us
    another operation x1, loops' own time, per_device(): lax.fori_loop(0, key_piece.shape[1] // KEY_BLOCK, one_block, start_states)  40.1 us
    slice x64, local copies, waits for them, and re-layouts, one_block(): group_pos[-1]  37.7 us
    all_gather x3, blocking collectives, prefix_by_axis(): lax.all_gather(part.astype(kind), axis)  28.3 us
    mul x64, local copies, waits for them, and re-layouts, update(): jnp.einsum('mqd,mkd->mqk', group_query, key_rows, preferred_element_type=...  20.7 us
    dot_general x8, matrix products, per_device(): jnp.dot(whole, weight, preferred_element_type=jnp.float32)  19.2 us
  transfers between devices with their start and end apart: 5, of which 0 were waited for; matrix products, arithmetic and copies ran while one was open for 12% of the time, Pallas kernels for 0%

profile of v1, /device:TPU:127, one launch (start us, length us, event | category | flops | bytes accessed | tf_op | source)
XLA Modules:
  0.0 742.9 jit_solution(6961739316583778211)
XLA Ops:
  18.0 5.5 all_to_all.48
  31.5 5.3 stack.2
  36.8 6.5 all-to-all-start.1
  54.3 144.3 %all-reduce.1 = bf16[32]{0:T(256)(128)(2,1)S(1)} all-reduce(bf16[32]{0:T(256)(128)(2,1)S(1)} %dynamic-update-slice), channel_id=3, replica_groups=mesh['sp_0'=4,'sp_1'=4,'fs'=4,'tp'=2] {'sp_1'}, use_global_device_ids=true, to_apply=%add.1 | all-reduce | flops 32 | bytes 128
  198.7 8.1 %all-gather.4 = bf16[4,1,8]{2,1,0:T(2,128)(2,1)S(1)} all-gather(bf16[1,1,8]{2,1,0:T(2,128)(2,1)S(1)} %get-tuple-element.351), channel_id=1, replica_groups=mesh['sp_0'=4,'sp_1'=4,'fs'=4,'tp'=2] {'sp_0'}, dimensions={0}, use_global_device_ids=true | all-gather | bytes 80 | tf_op jit(solution)/shard_map/all_gather | solution.py:64
  227.1 7.2 while.31
  235.5 10.1 %all-gather.2 = bf16[32,64,128]{2,1,0:T(8,128)(2,1)S(1)} all-gather(bf16[8,64,128]{2,1,0:T(8,128)(2,1)S(1)} %convert_element_type.242), channel_id=4, replica_groups=mesh['sp_0'=4,'sp_1'=4,'fs'=4,'tp'=2] {'sp_1'}, dimensions={0}, use_global_device_ids=true | all-gather | bytes 655360 | tf_op jit(solution)/shard_map/all_gather | solution.py:64
  246.5 10.2 %all_gather.38 = bf16[4,8,64,128]{3,2,1,0:T(8,128)(2,1)S(1)} all-gather(bf16[1,8,64,128]{3,2,1,0:T(8,128)(2,1)S(1)} %fusion.62), channel_id=1, replica_groups=mesh['sp_0'=4,'sp_1'=4,'fs'=4,'tp'=2] {'sp_0'}, dimensions={0}, use_global_device_ids=true | all-gather | bytes 655360 | tf_op jit(solution)/shard_map/all_gather | solution.py:64
  278.7 14.5 %all-to-all-start.3 = ((bf16[2,256,512]{1,2,0:T(8,128)(2,1)}), bf16[2,256,512]{1,2,0:T(8,128)(2,1)S(1)}, u32[]{:S(2)}, u32[]{:S(2)}) async-start(bf16[2,256,512]{1,2,0:T(8,128)(2,1)} %copy.128), calls=%async_computation.3 | async-start | bytes 1048576 | tf_op jit(solution)/shard_map/all_to_all | solution.py:275
  293.2 7.7 %copy.112 = bf16[16,4,512,128]{3,2,0,1:T(8,128)(2,1)} copy(bf16[16,4,512,128]{3,2,1,0:T(8,128)(2,1)} %all-to-all-done.1) | data formatting | bytes 16777216 | tf_op jit(solution)/shard_map/all_to_all | solution.py:23
  307.3 416.1 %while.30 = (s32[]{:T(128)}, f32[2,2,512]{2,1,0:T(2,128)S(1)}, f32[2,2,512]{2,1,0:T(2,128)S(1)}, f32[2,2,512,256]{3,2,1,0:T(8,128)}, s32[512]{0:T(512)S(1)}, /*i...) while((s32[]{:T(128)}, f32[2,2,512]{2,1,0:T(2,128)S(1)}, ...), condition=%wide.region_7.8_spmd, body=%wide.region_2.7_spmd.sunk | while | flops 204804224 | bytes 10801461 | solution.py:182
  315.0 5.3 conditional.2
  328.0 5.3 conditional.2
  334.5 5.3 conditional.2
  341.0 5.3 conditional.2
  354.0 5.3 conditional.2
  367.0 5.3 conditional.2
  380.0 5.3 conditional.2
  386.5 5.3 conditional.2
  393.0 5.3 conditional.2
  406.0 5.3 conditional.2
  419.0 5.3 conditional.2
  432.0 5.3 conditional.2
  438.5 5.3 conditional.2
  445.0 5.3 conditional.2
  458.0 5.3 conditional.2
  471.0 5.3 conditional.2
  484.0 5.3 conditional.2
  490.5 5.3 conditional.2
  497.0 5.3 conditional.2
  510.0 5.3 conditional.2
  523.0 5.3 conditional.2
  529.5 5.3 conditional.2
  536.0 5.3 conditional.2
  549.0 5.3 conditional.2
  562.0 5.3 conditional.2
  575.0 5.3 conditional.2
  588.0 5.3 conditional.2
  601.0 5.3 conditional.2
  614.1 5.3 conditional.2
  627.1 5.3 conditional.2
  640.1 5.3 conditional.2
  653.1 5.3 conditional.2
  666.1 5.3 conditional.2
  679.1 5.3 conditional.2
  692.1 5.3 conditional.2
  705.1 5.3 conditional.2
  718.1 5.3 conditional.2
  (1154 shorter events, 613.8 us)
Async XLA Ops:
  6.5 262.6 %copy-start = (bf16[2048,512]{1,0:T(8,128)(2,1)S(1)}, bf16[2048,512]{1,0:T(8,128)(2,1)}, u32[]{:S(2)}) copy-start(bf16[2048,512]{1,0:T(8,128)(2,1)} %param.31) | copy-start | bytes 6291460
  6.5 294.4 %all-gather.10.cloned.1.call-start = ((), (), s32[]{:S(2)}) async-start(), calls=%async_computation.5 | async-start | bytes 12582912 | tf_op jit(solution)/shard_map/all_gather | solution.py:81
  11.4 0.7 copy-start.21
  11.4 1.2 copy-start.4
  11.4 294.3 %all-gather.8.cloned.1.call-start = ((), (), s32[]{:S(2)}) async-start(), calls=%async_computation.4 | async-start | bytes 8912896 | tf_op jit(solution)/shard_map/all_gather | solution.py:145
  18.0 6.8 copy-start.25
  23.5 1.3 copy-start.2
  36.8 6.5 copy-start.27
  36.8 242.0 %all-to-all-start.1 = ((bf16[16,4,512,128]{3,2,1,0:T(8,128)(2,1)}), bf16[16,4,512,128]{3,2,1,0:T(8,128)(2,1)}, u32[]{:S(2)}, u32[]{:S(2)}) async-start(bf16[16,4,512,128]{3,2,1,0:T(8,128)(2,1)} %stack.2), calls=%async_computation.1 | async-start | bytes 16777216 | tf_op jit(solution)/shard_map/all_to_all | solution.py:23
  43.2 2.5 copy-start.3
  43.2 2.5 copy-start.28
  45.8 3.0 copy-start.8
  45.8 1.7 copy-start.26
  47.5 1.3 copy-start.9
  47.5 3.5 copy-start.29
  47.5 3.5 copy-start.14
  48.8 2.6 copy-start.15
  48.8 3.8 copy-start.30
  48.8 159.2 %copy-start.18 = (bf16[4,512]{1,0:T(4,128)(2,1)S(1)}, bf16[4,512]{1,0:T(4,128)(2,1)}, u32[]{:S(2)}) copy-start(bf16[4,512]{1,0:T(4,128)(2,1)} %param.36) | copy-start | bytes 12292
  48.8 159.2 %copy-start.19 = (bf16[4,256]{1,0:T(4,128)(2,1)S(1)}, bf16[4,256]{1,0:T(4,128)(2,1)}, u32[]{:S(2)}) copy-start(bf16[4,256]{1,0:T(4,128)(2,1)} %param.38) | copy-start | bytes 6148
  48.8 159.2 %copy-start.20 = (bf16[4,256]{1,0:T(4,128)(2,1)S(1)}, bf16[4,256]{1,0:T(4,128)(2,1)}, u32[]{:S(2)}) copy-start(bf16[4,256]{1,0:T(4,128)(2,1)} %param.37) | copy-start | bytes 6148
  49.7 166.6 %collective-permute-start = (bf16[3,1024]{0,1:T(8,128)(2,1)}, bf16[3,1024]{0,1:T(8,128)(2,1)}, u32[]{:S(2)}, u32[]{:S(2)}) collective-permute-start(bf16[3,1024]{0,1:T(8,128)(2,1)} %pad_maximum_fusion.1), channel_id=1, source_target_pairs={{0,8},{8,16},{16,24},{24,32},{32,40},{40,48},{48,56},{56,64},{64,7... | collective-permute-start | bytes 18440 | tf_op jit(solution)/shard_map/ppermute | solution.py:49
  51.4 162.9 %copy-start.10 = (f32[512,8]{0,1:T(8,128)}, f32[512,8]{0,1:T(8,128)S(1)}, u32[]{:S(2)}) copy-start(f32[512,8]{0,1:T(8,128)S(1)} %compare_select_fusion) | copy-start | bytes 49156
  257.8 1.0 copy-start.5
  257.8 1.0 copy-start.11
  257.9 1.0 copy-start.16
  258.9 1.2 copy-start.7
  258.9 1.2 copy-start.13
  258.9 1.2 copy-start.17
  276.2 1.2 copy-start.6
  276.3 1.2 copy-start.22
  278.7 22.2 %all-to-all-start.3 = ((bf16[2,256,512]{1,2,0:T(8,128)(2,1)}), bf16[2,256,512]{1,2,0:T(8,128)(2,1)S(1)}, u32[]{:S(2)}, u32[]{:S(2)}) async-start(bf16[2,256,512]{1,2,0:T(8,128)(2,1)} %copy.128), calls=%async_computation.3 | async-start | bytes 1048576 | tf_op jit(solution)/shard_map/all_to_all | solution.py:275
  305.7 1.5 copy-start.12
  307.3 416.1 %copy-start.24 = (f32[2]{0:T(128)S(1)}, f32[2]{0:T(128)}, u32[]{:S(2)}) copy-start(f32[2]{0:T(128)} %param.41) | copy-start | bytes 28
  723.4 2.1 copy-start.23
  730.8 5.3 copy-start.1
Sparse Core Ops, SparseCore 0:
  11.5 24.0 all-gather.9
  37.7 175.0 all-gather.7
